TPU v7x, 256 devices: a whole 4x4x8 slice. The times are simulated.
256 devices in a mesh: sp: 64 (over z, y, core), tp: 4 (over x).
Axes of the slice: x: 4, y: 4, z: 8, core: 2. Of those that a mesh axis runs over, the one named last changes fastest.
Arguments:
- queries: bfloat16 [32768, 1024], P('sp', 'tp'), may hold values from -6 to 6
- keys: bfloat16 [32768, 1024], P('sp', 'tp'), may hold values from -6 to 6
- values: bfloat16 [32768, 1024], P('sp', 'tp'), may hold values from -6 to 6
- output_gate_logits: bfloat16 [32768, 1024], P('sp', 'tp'), may hold values from -6 to 6
- input_gate_log: float32 [32768, 8], P('sp', 'tp'), may hold values from -5 to 125
- forget_gate_logits: float32 [32768, 8], P('sp', 'tp')
- extra_decay_log: float32 [32768, 8], P('sp', 'tp'), may hold values from -1 to 0
- document: int32 [32768], P('sp'), may hold values from 0 to 31, never falling along the last dimension, each value on 1 to 2048 neighbouring positions
- residual: bfloat16 [32768, 2048], P('sp', 'tp'), may hold values from -16 to 16
- cell_norm_gain: bfloat16 [1024], P('tp'), may hold values from 0.099609375 to 1.8984375
- output_weight: bfloat16 [1024, 2048], P('tp'), may hold values from -0.1875 to 0.1875
- mixer_norm_gain: bfloat16 [2048], P('tp'), may hold values from 0.099609375 to 1.8984375
- up_weight: bfloat16 [2048, 8192], P('sp', 'tp'), may hold values from -0.125 to 0.125
- down_weight: bfloat16 [8192, 2048], P('tp', 'sp'), may hold values from -0.0625 to 0.0625
Outputs:
- layer_out: bfloat16 [32768, 2048], P('sp', 'tp')
All inputs are finite; a program needn't handle non-finite values.
Results may differ from a plain program's by a relative error of at most 0.015.
Values may be sent and summed in bfloat16 or wider, within the bound.
No kernel may reach another device: no remote copies, remote signals or barrier semaphores. Data moves between devices by JAX's collectives and lax.ppermute only.
A program may use at most 128 MiB of HBM per device.

v0:
```python
import jax
import jax.numpy as jnp
from jax import lax
from jax.sharding import Mesh
from jax.sharding import PartitionSpec as P

DH = 128
BLOCK = 128
SP = ("sp_0", "sp_1", "sp_2")
NEG = -1e30
EPS = 1e-06


def sent_to_all(value, axis):
    copies = jnp.broadcast_to(value, (lax.axis_size(axis), *value.shape))
    return lax.all_to_all(copies, axis, split_axis=0, concat_axis=0, tiled=True)


def of_everyone(value, axis):
    return sent_to_all(value, axis).sum(axis=0)


def rows_first(arrays, axis, dims):
    turned = [jnp.moveaxis(a, dim, 0) for a, dim in zip(arrays, dims)]
    widths = [t[0].size for t in turned]
    both = jnp.concatenate([t.reshape(-1, w) for t, w in zip(turned, widths)], axis=1)
    whole = lax.all_gather(both, axis, axis=0, tiled=True)
    parts = jnp.split(whole, [sum(widths[:k]) for k in range(1, len(widths))], axis=1)
    return tuple(
        (
            jnp.moveaxis(b.reshape(-1, *t.shape[1:]), 0, dim)
            for b, t, dim in zip(parts, turned, dims)
        )
    )


def nothing_yet(value, identity):
    return jax.tree.map(
        lambda a, e: jnp.broadcast_to(jnp.asarray(e, a.dtype), a.shape), value, identity
    )


def all_in_one(value, axis):
    leaves = jax.tree.leaves(value)
    order = sorted(range(len(leaves)), key=lambda k: -leaves[k].size)
    width = (1, *leaves[order[0]].shape)[-1]
    lines = [
        jnp.pad(leaves[k].reshape(-1), (0, -leaves[k].size % width)).reshape(-1, width)
        for k in order
    ]
    both, at, found = (lax.all_gather(jnp.concatenate(lines), axis), 0, {})
    for k, line in zip(order, lines):
        piece = both[:, at : at + len(line)].reshape(len(both), -1)
        found[k] = piece[:, : leaves[k].size].reshape(-1, *leaves[k].shape)
        at += len(line)
    numbers = iter(range(len(leaves)))
    return jax.tree.map(lambda _: found[next(numbers)], value)


def collected_alike(value, axis):
    leaves, found = (jax.tree.leaves(value), {})
    for leading, a in enumerate(leaves):
        if leading not in found:
            alike = [k for k, b in enumerate(leaves) if b.dtype == a.dtype]
            got = (
                all_in_one([leaves[k] for k in alike], axis)
                if len(alike) > 1
                else [lax.all_gather(a, axis)]
            )
            for k, b in zip(alike, got):
                found[k] = b
    numbers = iter(range(len(leaves)))
    return jax.tree.map(lambda _: found[next(numbers)], value)


def entering(value, axes, combine, identity):
    before = start = nothing_yet(value, identity)
    subtotal = value
    for axis in reversed(axes):
        count, index = (lax.axis_size(axis), lax.axis_index(axis))
        pieces = collected_alike(subtotal, axis)
        inside, subtotal = (start, start)
        for k in range(count):
            passed = k < index
            subtotal = combine(subtotal, jax.tree.map(lambda part: part[k], pieces))
            inside = jax.tree.map(lambda new, old: jnp.where(passed, new, old), subtotal, inside)
        before = combine(inside, before)
    return before


def cut_along(value, dim, count):
    lengths = value.shape
    parts = value.reshape(*lengths[:dim], count, lengths[dim] // count, *lengths[dim + 1 :])
    return jnp.moveaxis(parts, dim, 0)


def summed_on_arrival(value, axis, dim):
    parts = cut_along(value, dim, lax.axis_size(axis))
    arrived = lax.all_to_all(parts, axis, split_axis=0, concat_axis=0, tiled=True)
    return arrived.astype(jnp.float32).sum(axis=0)


def joined_along(parts, dim):
    parts = jnp.moveaxis(parts, 0, dim)
    lengths = parts.shape
    return parts.reshape(*lengths[:dim], lengths[dim] * lengths[dim + 1], *lengths[dim + 2 :])


def gathered_copies(value, axis, dim):
    return joined_along(sent_to_all(value, axis), dim)


def block_terms(carry, inputs):
    memory, normer, stabil, last_doc = carry
    q_blk, k_blk, v_blk, gate_in, gate_log, doc_blk = inputs
    length = doc_blk.shape[0]
    causal = jnp.arange(length)[:, None] >= jnp.arange(length)[None, :]
    cumulative = jnp.cumsum(gate_log, axis=-1)
    same_doc = (doc_blk[:, None] == doc_blk[None, :]) & causal
    pair_log = cumulative[:, :, None] - cumulative[:, None, :] + gate_in[:, None, :]
    pair_log = jnp.where(same_doc[None], pair_log, NEG)
    live_rows = doc_blk == last_doc
    carried_log = jnp.where(live_rows[None, :], cumulative + stabil[:, None], NEG)
    peak_log = jnp.maximum(carried_log, jnp.max(pair_log, axis=-1))
    weights = jnp.exp(pair_log - peak_log[:, :, None])
    carried = jnp.exp(carried_log - peak_log)
    scores = jnp.einsum("htd,hsd->hts", q_blk, k_blk) * weights
    numerator = carried[:, :, None] * jnp.einsum("htd,hde->hte", q_blk, memory)
    numerator = numerator + jnp.einsum("hts,hse->hte", scores, v_blk)
    denominator = carried * jnp.einsum("htd,hd->ht", q_blk, normer) + jnp.sum(scores, axis=-1)
    end_doc = doc_blk[-1]
    end_cum = cumulative[:, -1]
    keep_log = jnp.where(
        (doc_blk == end_doc)[None, :], end_cum[:, None] - cumulative + gate_in, NEG
    )
    old_log = jnp.where(last_doc == end_doc, end_cum + stabil, NEG)
    new_stab = jnp.maximum(old_log, jnp.max(keep_log, axis=-1))
    scaled = jnp.exp(keep_log - new_stab[:, None])
    decayed = jnp.exp(old_log - new_stab)
    memory = decayed[:, None, None] * memory + jnp.einsum("hs,hsd,hse->hde", scaled, k_blk, v_blk)
    normer = decayed[:, None] * normer + jnp.einsum("hs,hsd->hd", scaled, k_blk)
    return ((memory, normer, new_stab, end_doc), (numerator, denominator, peak_log, cumulative))


def split_heads(source, blocks):
    return source.astype(jnp.float32).reshape(blocks, BLOCK, -1, DH).transpose(0, 2, 1, 3)


def split_gates(source, blocks):
    return source.reshape(blocks, BLOCK, -1).transpose(0, 2, 1)


def within_block_pass(
    queries, keys, values, input_gate_log, forget_gate_logits, extra_decay_log, document
):
    blocks = queries.shape[0] // BLOCK
    head_count = queries.shape[1] // DH
    query_heads = split_heads(queries, blocks) * DH ** (-0.5)
    forget_log_values = jax.nn.log_sigmoid(forget_gate_logits) + extra_decay_log
    inputs = (
        query_heads,
        split_heads(keys, blocks),
        split_heads(values, blocks),
        split_gates(input_gate_log, blocks),
        split_gates(forget_log_values, blocks),
        document.reshape(blocks, BLOCK),
    )
    initial = (
        jnp.zeros((head_count, DH, DH), jnp.float32),
        jnp.zeros((head_count, DH), jnp.float32),
        jnp.full((head_count,), NEG, jnp.float32),
        jnp.array(-1, jnp.int32),
    )
    final_state, output_rows = lax.scan(block_terms, initial, inputs)
    return (query_heads, final_state, output_rows)


def head_mix(cell_out, output_gate_logits, cell_norm_gain):
    row_count = output_gate_logits.shape[0]
    head_count = cell_out.shape[1]
    hidden = cell_out.transpose(0, 2, 1, 3).reshape(row_count, head_count * DH)
    squares = of_everyone(jnp.sum(hidden * hidden, axis=1), "tp")
    inverse = lax.rsqrt(squares / (head_count * DH * lax.axis_size("tp")) + EPS)
    gated = jax.nn.sigmoid(output_gate_logits.astype(jnp.float32))
    gains = cell_norm_gain.astype(jnp.float32)
    return (gated * hidden * inverse[:, None] * gains[None, :]).astype(jnp.bfloat16)


def join_states(earlier, later):
    mem_a, norm_a, stab_a, log_a, first_a, last_a = earlier
    mem_b, norm_b, stab_b, log_b, first_b, last_b = later
    joined = last_a == last_b
    stab_ab = jnp.where(joined, jnp.maximum(log_b + stab_a, stab_b), stab_b)
    weight_a = jnp.where(joined, jnp.exp(log_b + stab_a - stab_ab), 0.0)
    weight_b = jnp.exp(stab_b - stab_ab)
    memory = weight_a[:, None, None] * mem_a + weight_b[:, None, None] * mem_b
    normer = weight_a[:, None] * norm_a + weight_b[:, None] * norm_b
    blank_b = last_b < 0
    memory = jnp.where(blank_b, mem_a, memory)
    normer = jnp.where(blank_b, norm_a, normer)
    stabil = jnp.where(blank_b, stab_a, stab_ab)
    first_doc = jnp.where(first_a < 0, first_b, first_a)
    last_doc = jnp.where(blank_b, last_a, last_b)
    return (memory, normer, stabil, log_a + log_b, first_doc, last_doc)


def local(
    queries,
    keys,
    values,
    output_gate_logits,
    input_gate_log,
    forget_gate_logits,
    extra_decay_log,
    document,
    residual,
    cell_norm_gain,
    output_weight,
    mixer_norm_gain,
    up_weight,
    down_weight,
):
    up_whole, down_whole = rows_first((up_weight, down_weight), SP, (0, 1))
    query_heads, final_state, output_rows = within_block_pass(
        queries, keys, values, input_gate_log, forget_gate_logits, extra_decay_log, document
    )
    numerator, denominator, peak_log, cumulative = output_rows
    memory, normer, stabil, last_doc = final_state
    step_logs = cumulative[:, :, -1]
    offsets = jnp.cumsum(step_logs, axis=0) - step_logs
    through = cumulative + offsets[:, :, None]
    summary = (memory, normer, stabil, jnp.sum(step_logs, axis=0), document[0], last_doc)
    identity = (
        jnp.zeros_like(memory),
        jnp.zeros_like(normer),
        jnp.full_like(stabil, NEG),
        jnp.zeros_like(stabil),
        jnp.array(-1, jnp.int32),
        jnp.array(-1, jnp.int32),
    )
    prefix = entering(summary, SP, join_states, identity)
    doc_blocks = document.reshape(-1, BLOCK)
    carried_log = jnp.where(
        (doc_blocks == prefix[5])[:, None, :], through + prefix[2][None, :, None], NEG
    )
    merged_peak = jnp.maximum(peak_log, carried_log)
    own_weight = jnp.exp(peak_log - merged_peak)
    far_weight = jnp.exp(carried_log - merged_peak)
    numerator = own_weight[..., None] * numerator + far_weight[..., None] * jnp.einsum(
        "nhtd,hde->nhte", query_heads, prefix[0]
    )
    denominator = own_weight * denominator + far_weight * jnp.einsum(
        "nhtd,hd->nht", query_heads, prefix[1]
    )
    cell_out = numerator / jnp.maximum(jnp.abs(denominator), 1.0)[..., None]
    mixed = head_mix(cell_out, output_gate_logits, cell_norm_gain)
    head_terms = jnp.dot(mixed, output_weight, preferred_element_type=jnp.float32)
    width = residual.shape[1]
    model_width = width * lax.axis_size("tp")
    own_sum = summed_on_arrival(head_terms.astype(jnp.bfloat16), "tp", 1)
    first_sum = (residual.astype(jnp.float32) + own_sum).astype(jnp.bfloat16)
    first_wide = lax.optimization_barrier(first_sum).astype(jnp.float32)
    squares = of_everyone(jnp.sum(first_wide * first_wide, axis=1), "tp")
    inverse = lax.rsqrt(squares / model_width + EPS)
    normed_own = (first_wide * inverse[:, None] * mixer_norm_gain.astype(jnp.float32)).astype(
        jnp.bfloat16
    )
    normed_full = gathered_copies(normed_own, "tp", 1)
    hidden = jnp.dot(normed_full, up_whole, preferred_element_type=jnp.float32)
    squared = jnp.square(jax.nn.relu(hidden)).astype(jnp.bfloat16)
    channel = jnp.dot(squared, down_whole, preferred_element_type=jnp.float32)
    own_channel = summed_on_arrival(channel.astype(jnp.bfloat16), "tp", 1)
    return (lax.optimization_barrier(first_sum).astype(jnp.float32) + own_channel).astype(
        jnp.bfloat16
    )


def solution(mesh):
    split = Mesh(mesh.devices.reshape(8, 4, 2, mesh.shape["tp"]), ("sp_0", "sp_1", "sp_2", "tp"))
    return jax.shard_map(
        local,
        mesh=split,
        in_specs=(
            P(SP, "tp"),
            P(SP, "tp"),
            P(SP, "tp"),
            P(SP, "tp"),
            P(SP, "tp"),
            P(SP, "tp"),
            P(SP, "tp"),
            P(SP),
            P(SP, "tp"),
            P("tp"),
            P("tp", None),
            P("tp"),
            P(SP, "tp"),
            P("tp", SP),
        ),
        out_specs=P(SP, "tp"),
        check_vma=False,
    )
```

profile of v0, /device:TPU:1, one launch (start us, length us, event | category | flops | bytes accessed | tf_op | source)
XLA Modules:
  0.0 278.6 jit_solution(83311342895520995)
XLA Ops:
  6.7 1.1 convert_multiply_fusion.2
  7.8 1.2 reshape.3525
  9.0 1.0 reshape.3526
  10.6 25.0 %while.25 = (s32[]{:T(128)}, f32[2,128,128]{2,1,0:T(8,128)S(1)}, f32[2,128]{1,0:T(2,128)S(1)}, f32[2]{0:T(128)S(1)}, s32[]{:T(128)}, /*index=5*/f32[4,2,128,128]...) while((s32[]{:T(128)}, f32[2,128,128]{2,1,0:T(8,128)S(1)}, ...), condition=%wide.region_5.6_spmd.clone, body=%wide.region_0.5_spmd.clone.sunk | while | flops 34361868 | bytes 2780512 | solution.py:174
  12.3 0.9 fusion.317
  15.3 0.7 constant_dynamic-update-slice_fusion.7
  18.5 0.9 fusion.317
  21.6 0.7 constant_dynamic-update-slice_fusion.7
  24.8 0.9 fusion.317
  27.8 0.7 constant_dynamic-update-slice_fusion.7
  31.0 0.9 fusion.317
  34.0 0.7 constant_dynamic-update-slice_fusion.7
  35.6 0.7 dynamic-slice
  37.0 0.7 fusion.253
  37.7 4.7 %all-reduce.6 = s32[4]{0:T(128)S(1)} all-reduce(s32[4]{0:T(128)S(1)} %fusion.253), channel_id=2, replica_groups=mesh['sp_0'=8,'sp_1'=4,'sp_2'=2,'tp'=4] {'sp_2'}, use_global_device_ids=true, to_apply=%add.6 | all-reduce | flops 4 | bytes 32
  49.9 5.4 %all-reduce.7 = s32[8]{0:T(128)S(1)} all-reduce(s32[8]{0:T(128)S(1)} %fusion.254), channel_id=3, replica_groups=mesh['sp_0'=8,'sp_1'=4,'sp_2'=2,'tp'=4] {'sp_1'}, use_global_device_ids=true, to_apply=%add.7 | all-reduce | flops 8 | bytes 64
  55.3 0.7 fusion.287
  57.4 4.0 %all-gather.6 = f32[2,260,128]{2,1,0:T(8,128)S(1)} all-gather(f32[1,260,128]{2,1,0:T(8,128)S(1)} %maximum_bitcast_fusion), channel_id=5, replica_groups=mesh['sp_0'=8,'sp_1'=4,'sp_2'=2,'tp'=4] {'sp_2'}, dimensions={0}, use_global_device_ids=true | all-gather | bytes 399360 | tf_op jit(solution)/shard_map/all_gather | solution.py:51
  61.8 9.9 %all-gather.7 = f32[4,260,128]{2,1,0:T(8,128)S(1)} all-gather(f32[1,260,128]{2,1,0:T(8,128)S(1)} %maximum_bitcast_fusion.1), channel_id=6, replica_groups=mesh['sp_0'=8,'sp_1'=4,'sp_2'=2,'tp'=4] {'sp_1'}, dimensions={0}, use_global_device_ids=true | all-gather | bytes 665600 | tf_op jit(solution)/shard_map/all_gather | solution.py:51
  77.8 0.7 maximum_bitcast_fusion.2
  78.6 0.7 pad_maximum_fusion
  82.5 0.6 dynamic-slice.2
  84.4 13.2 %all-reduce.8 = s32[16]{0:T(128)S(1)} all-reduce(s32[16]{0:T(128)S(1)} %fusion.255), channel_id=4, replica_groups=mesh['sp_0'=8,'sp_1'=4,'sp_2'=2,'tp'=4] {'sp_0'}, use_global_device_ids=true, to_apply=%add.8 | all-reduce | flops 16 | bytes 128
  97.7 0.7 fusion.286
  114.1 0.8 copy.162
  114.8 0.7 copy.163
  115.6 0.8 copy.164
  116.3 0.7 copy.165
  117.3 1.4 fusion.280
  118.6 0.7 copy.152
  119.4 0.7 copy.153
  120.1 0.8 copy.154
  121.4 0.8 fusion.281
  122.5 0.9 add_select_fusion.4
  123.7 2.1 multiply_reduce_fusion
  126.4 3.9 %all-to-all-start = ((f32[4,1,512]{2,1,0:T(1,128)}), f32[4,1,512]{2,1,0:T(1,128)S(1)}, u32[]{:S(2)}, u32[]{:S(2)}) async-start(f32[4,1,512]{2,1,0:T(1,128)} %broadcast_in_dim.110), calls=%async_computation | async-start | bytes 16384 | tf_op jit(solution)/shard_map/all_to_all | solution.py:16
  130.5 3.9 %all-to-all-done = f32[4,1,512]{2,1,0:T(1,128)S(1)} async-done(((f32[4,1,512]{2,1,0:T(1,128)}), f32[4,1,512]{2,1,0:T(1,128)S(1)}, u32[]{:S(2)}, u32[]{:S(2)}) %all-to-all-start) | async-done | bytes 8224 | tf_op jit(solution)/shard_map/all_to_all | solution.py:16
  134.5 1.7 convolution_convert_fusion
  136.4 20.6 %all_to_all.27 = bf16[4,512,512]{2,1,0:T(8,128)(2,1)S(1)} all-to-all(bf16[4,512,512]{2,1,0:T(8,128)(2,1)S(1)} %bitcast.687), channel_id=1, replica_groups=mesh['sp_0'=8,'sp_1'=4,'sp_2'=2,'tp'=4] {'tp'}, dimensions={0} | all-to-all | bytes 4194304 | tf_op jit(solution)/shard_map/all_to_all | solution.py:99
  157.4 0.7 copy-done.1
  159.0 3.2 %all-to-all-start.2 = ((f32[4,1,512]{2,1,0:T(1,128)}), f32[4,1,512]{2,1,0:T(1,128)S(1)}, u32[]{:S(2)}, u32[]{:S(2)}) async-start(f32[4,1,512]{2,1,0:T(1,128)} %broadcast_in_dim.111), calls=%async_computation.2 | async-start | bytes 16384 | tf_op jit(solution)/shard_map/all_to_all | solution.py:16
  162.3 4.1 %all-to-all-done.2 = f32[4,1,512]{2,1,0:T(1,128)S(1)} async-done(((f32[4,1,512]{2,1,0:T(1,128)}), f32[4,1,512]{2,1,0:T(1,128)S(1)}, u32[]{:S(2)}, u32[]{:S(2)}) %all-to-all-start.2) | async-done | bytes 8224 | tf_op jit(solution)/shard_map/all_to_all | solution.py:16
  167.1 19.4 %all_to_all.28 = bf16[4,512,512]{1,2,0:T(8,128)(2,1)} all-to-all(bf16[4,512,512]{1,2,0:T(8,128)(2,1)S(1)} %broadcast_in_dim.112), channel_id=1, replica_groups=mesh['sp_0'=8,'sp_1'=4,'sp_2'=2,'tp'=4] {'tp'}, dimensions={0} | all-to-all | bytes 4194304 | tf_op jit(solution)/shard_map/all_to_all | solution.py:16
  186.5 35.9 %all-gather.12.cloned.1.call-done = bf16[2048,4096]{1,0:T(8,128)(2,1)} async-done(((bf16[32,4096]{1,0:T(8,128)(2,1)}), bf16[2048,4096]{1,0:T(8,128)(2,1)}) %all-gather.12.cloned.1.call-update) | async-done | bytes 16777232 | tf_op jit(solution)/shard_map/all_gather | solution.py:27
  222.4 16.6 %fusion.24 = bf16[512,2048]{1,0:T(8,128)(2,1)} fusion(bf16[2048,4096]{1,0:T(8,128)(2,1)} %all-gather.12.cloned.1.call-done, bf16[512,2048]{0,1:T(8,128)(2,1)} %bitcast.691), kind=kOutput, calls=%fused_computation.56 | convolution fusion | flops 8594128896 | bytes 20971520 | tf_op jit(solution)/shard_map/dot_general | solution.py:271
  239.0 1.8 copy.230
  240.8 29.7 %all_to_all.29 = bf16[4,512,512]{2,1,0:T(8,128)(2,1)S(1)} all-to-all(bf16[4,512,512]{2,1,0:T(8,128)(2,1)S(1)} %bitcast.688), channel_id=1, replica_groups=mesh['sp_0'=8,'sp_1'=4,'sp_2'=2,'tp'=4] {'tp'}, dimensions={0} | all-to-all | bytes 4194304 | tf_op jit(solution)/shard_map/all_to_all | solution.py:99
  270.8 1.0 fusion.37
  (206 shorter events, 22.6 us)
Async XLA Ops:
  6.5 127.9 %copy-start = (bf16[256,2048]{1,0:T(8,128)(2,1)S(1)}, bf16[256,2048]{1,0:T(8,128)(2,1)}, u32[]{:S(2)}) copy-start(bf16[256,2048]{1,0:T(8,128)(2,1)} %param.26) | copy-start | bytes 3145732
  6.5 3.5 %copy-start.6 = (s32[512]{0:T(512)S(1)}, s32[512]{0:T(512)}, u32[]{:S(2)}) copy-start(s32[512]{0:T(512)} %param.23) | copy-start | bytes 6148
  6.5 4.0 %copy-start.8 = (f32[512,2]{0,1:T(2,128)S(1)}, f32[512,2]{0,1:T(2,128)}, u32[]{:S(2)}) copy-start(f32[512,2]{0,1:T(2,128)} %param.21) | copy-start | bytes 12292
  6.5 4.0 %copy-start.7 = (f32[512,2]{0,1:T(2,128)S(1)}, f32[512,2]{0,1:T(2,128)}, u32[]{:S(2)}) copy-start(f32[512,2]{0,1:T(2,128)} %param.22) | copy-start | bytes 12292
  6.5 110.7 %all-gather.14.cloned.1.call-start = ((), (), s32[]{:S(2)}) async-start(), calls=%async_computation.6 | async-start | bytes 1216512 | tf_op jit(solution)/shard_map/all_gather | solution.py:51
  10.6 25.1 %copy-start.13 = (u32[256]{0:T(256)S(1)}, u32[256]{0:T(256)}, u32[]{:S(2)}) copy-start(u32[256]{0:T(256)} %constant.114) | copy-start | bytes 3076
  10.6 35.4 %copy-start.12 = (u32[256]{0:T(256)S(1)}, u32[256]{0:T(256)}, u32[]{:S(2)}) copy-start(u32[256]{0:T(256)} %constant.119) | copy-start | bytes 3076
  35.6 42.9 %copy-start.4 = (bf16[2048,32]{0,1:T(8,128)(2,1)S(1)}, bf16[2048,32]{0,1:T(8,128)(2,1)}, u32[]{:S(2)}) copy-start(bf16[2048,32]{0,1:T(8,128)(2,1)} %param.29) | copy-start | bytes 393220
  35.6 42.9 %copy-start.5 = (bf16[32,2048]{1,0:T(8,128)(2,1)S(1)}, bf16[32,2048]{1,0:T(8,128)(2,1)}, u32[]{:S(2)}) copy-start(bf16[32,2048]{1,0:T(8,128)(2,1)} %param.28) | copy-start | bytes 393220
  49.2 33.3 %copy-start.11 = (u32[256]{0:T(256)S(1)}, u32[256]{0:T(256)}, u32[]{:S(2)}) copy-start(u32[256]{0:T(256)} %constant.124) | copy-start | bytes 3076
  78.5 143.9 %all-gather.12.cloned.1.call-start = ((), (), s32[]{:S(2)}) async-start(), calls=%async_computation.5 | async-start | bytes 17039360 | tf_op jit(solution)/shard_map/all_gather | solution.py:27
  119.4 4.3 %copy-start.2 = (f32[2,128,128]{1,2,0:T(8,128)S(1)}, f32[2,128,128]{1,2,0:T(8,128)}, u32[]{:S(2)}) copy-start(f32[2,128,128]{1,2,0:T(8,128)} %copy.162) | copy-start | bytes 393220
  120.1 3.6 %copy-start.3 = (f32[2,128,128]{1,2,0:T(8,128)S(1)}, f32[2,128,128]{1,2,0:T(8,128)}, u32[]{:S(2)}) copy-start(f32[2,128,128]{1,2,0:T(8,128)} %copy.163) | copy-start | bytes 393220
  123.7 6.6 %copy-start.10 = (bf16[256]{0:T(256)(128)(2,1)S(1)}, bf16[256]{0:T(256)(128)(2,1)}, u32[]{:S(2)}) copy-start(bf16[256]{0:T(256)(128)(2,1)} %param.25) | copy-start | bytes 1540
  126.4 8.0 %all-to-all-start = ((f32[4,1,512]{2,1,0:T(1,128)}), f32[4,1,512]{2,1,0:T(1,128)S(1)}, u32[]{:S(2)}, u32[]{:S(2)}) async-start(f32[4,1,512]{2,1,0:T(1,128)} %broadcast_in_dim.110), calls=%async_computation | async-start | bytes 16384 | tf_op jit(solution)/shard_map/all_to_all | solution.py:16
  157.1 1.0 copy-start.1
  158.1 4.2 %copy-start.9 = (bf16[512]{0:T(512)(128)(2,1)S(1)}, bf16[512]{0:T(512)(128)(2,1)}, u32[]{:S(2)}) copy-start(bf16[512]{0:T(512)(128)(2,1)} %param.27) | copy-start | bytes 3076
  159.0 7.4 %all-to-all-start.2 = ((f32[4,1,512]{2,1,0:T(1,128)}), f32[4,1,512]{2,1,0:T(1,128)S(1)}, u32[]{:S(2)}, u32[]{:S(2)}) async-start(f32[4,1,512]{2,1,0:T(1,128)} %broadcast_in_dim.111), calls=%async_computation.2 | async-start | bytes 16384 | tf_op jit(solution)/shard_map/all_to_all | solution.py:16
Sparse Core Ops, SparseCore 0:
  78.6 38.6 all-gather.13
  120.0 102.3 all-gather.11
where the time goes:
time: 280 us; the launch traced here: 279 us
  blocking collectives  107 us (38%)
  between operations  46.7 us (17%)
  waiting for transfers between devices  44.1 us (16%)
  local copies, waits for them, and re-layouts  26.7 us (10%)
  matrix products  25.1 us (9%)
  other arithmetic  17 us (6%)
  starting transfers between devices  7.18 us (3%)
  loops' own time  4.89 us (2%)
    all_to_all x2, blocking collectives, summed_on_arrival(): lax.all_to_all(parts, axis, split_axis=0, concat_axis=0, tiled=True)  50.3 us
    all_gather x1, waiting for transfers between devices, rows_first(): whole = lax.all_gather(both, axis, axis=0, tiled=True)  35.9 us
    unnamed x3, blocking collectives  23.2 us
    all_to_all x1, blocking collectives, sent_to_all(): return lax.all_to_all(copies, axis, split_axis=0, concat_axis=0, tiled=True)  19.4 us
    dot_general x1, matrix products, local(): channel = jnp.dot(squared, down_whole, preferred_element_type=jnp.float32)  16.6 us
    all_gather x2, blocking collectives, all_in_one(): both, at, found = (lax.all_gather(jnp.concatenate(lines), axis), 0, {})  13.9 us
    all_to_all x2, waiting for transfers between devices, sent_to_all(): return lax.all_to_all(copies, axis, split_axis=0, concat_axis=0, tiled=True)  8.02 us
    all_to_all x2, starting transfers between devices, sent_to_all(): return lax.all_to_all(copies, axis, split_axis=0, concat_axis=0, tiled=True)  7.1 us
  transfers between devices with their start and end apart: 4, of which 4 were waited for; matrix products, arithmetic and copies ran while one was open for 7% of the time, Pallas kernels for 0%

commit v1 on v0

--- a/solution.py
+++ b/solution.py
@@ -11,6 +11,11 @@
 EPS = 1e-06
 
 
+def exchange_gather(value, axis, d):
+    sent = jnp.stack([value] * lax.axis_size(axis))
+    return jnp.concatenate(lax.all_to_all(sent, axis, 0, 0), axis=d)
+
+
 def sent_to_all(value, axis):
     copies = jnp.broadcast_to(value, (lax.axis_size(axis), *value.shape))
     return lax.all_to_all(copies, axis, split_axis=0, concat_axis=0, tiled=True)
@@ -24,7 +29,7 @@
     turned = [jnp.moveaxis(a, dim, 0) for a, dim in zip(arrays, dims)]
     widths = [t[0].size for t in turned]
     both = jnp.concatenate([t.reshape(-1, w) for t, w in zip(turned, widths)], axis=1)
-    whole = lax.all_gather(both, axis, axis=0, tiled=True)
+    whole = exchange_gather(both, axis, 0)
     parts = jnp.split(whole, [sum(widths[:k]) for k in range(1, len(widths))], axis=1)
     return tuple(
         (

time: 280 us -> 634 us (2.26)
  blocking collectives: 107 us -> 469 us
  waiting for transfers between devices: 44.1 us -> 27.2 us
    all_to_all x1, blocking collectives: 19.4 us -> 383 us  [exchange_gather(): return jnp.concatenate(lax.all_to_all(sent, axis, 0, 0), axis=d)]
    all_gather x1 -> x0, waiting for transfers between devices: 35.9 us -> none  [rows_first(): whole = lax.all_gather(both, axis, axis=0, tiled=True)]
    all_to_all x2 -> x3, waiting for transfers between devices: 8.02 us -> 24.9 us  [sent_to_all(): return lax.all_to_all(copies, axis, split_axis=0, concat_axis=0, tiled=True)]
  transfers between devices with their start and end apart: 4 -> 4, of which waited for: 4 -> 4; matrix products, arithmetic and copies ran while one was open for 7% -> 0% of each run, Pallas kernels for 0% -> 0%
where the time goes in v1:
time: 634 us; the launch traced here: 631 us
  blocking collectives  469 us (74%)
  between operations  47.9 us (8%)
  local copies, waits for them, and re-layouts  27.8 us (4%)
  waiting for transfers between devices  27.2 us (4%)
  matrix products  25 us (4%)
  other arithmetic  16.6 us (3%)
  starting transfers between devices  11.8 us (2%)
    all_to_all x1, blocking collectives, exchange_gather(): return jnp.concatenate(lax.all_to_all(sent, axis, 0, 0), axis=d)  383 us
    all_to_all x2, blocking collectives, summed_on_arrival(): lax.all_to_all(parts, axis, split_axis=0, concat_axis=0, tiled=True)  48.3 us
    all_to_all x3, waiting for transfers between devices, sent_to_all(): return lax.all_to_all(copies, axis, split_axis=0, concat_axis=0, tiled=True)  24.9 us
    unnamed x3, blocking collectives  23.2 us
    dot_general x1, matrix products, local(): channel = jnp.dot(squared, down_whole, preferred_element_type=jnp.float32)  16.6 us
    all_gather x2, blocking collectives, all_in_one(): both, at, found = (lax.all_gather(jnp.concatenate(lines), axis), 0, {})  13.9 us
  transfers between devices with their start and end apart: 4, of which 4 were waited for; matrix products, arithmetic and copies ran while one was open for 0% of the time, Pallas kernels for 0%

profile of v1, /device:TPU:1, one launch (start us, length us, event | category | flops | bytes accessed | tf_op | source)
XLA Modules:
  0.0 630.7 jit_solution(814193050342886054)
XLA Ops:
  6.7 1.3 reshape.3531
  7.9 1.0 reshape.3532
  9.0 1.0 convert_multiply_fusion.2
  10.7 26.0 %while.25 = (s32[]{:T(128)}, f32[2,128,128]{2,1,0:T(8,128)S(1)}, f32[2,128]{1,0:T(2,128)S(1)}, f32[2]{0:T(128)S(1)}, s32[]{:T(128)}, /*index=5*/f32[4,2,128,128]...) while((s32[]{:T(128)}, f32[2,128,128]{2,1,0:T(8,128)S(1)}, ...), condition=%wide.region_5.6_spmd.clone, body=%wide.region_0.5_spmd.clone.sunk | while | flops 34361868 | bytes 2780012 | solution.py:179
  12.6 0.9 fusion.317
  15.9 0.7 constant_dynamic-update-slice_fusion.7
  19.1 0.9 fusion.317
  22.4 0.7 constant_dynamic-update-slice_fusion.7
  25.0 0.6 compare_bitcast_fusion.5
  25.6 0.9 fusion.317
  28.9 0.7 constant_dynamic-update-slice_fusion.7
  32.1 0.9 fusion.317
  35.4 0.7 constant_dynamic-update-slice_fusion.7
  37.9 0.9 fusion.253
  38.8 4.7 all-reduce.6
  43.5 0.7 fusion.288
  46.8 0.7 dynamic-slice.1
  51.4 5.4 all-reduce.7
  56.9 0.7 fusion.287
  59.0 4.0 all-gather.6
  63.4 9.9 %all-gather.7 = f32[4,260,128]{2,1,0:T(8,128)S(1)} all-gather(f32[1,260,128]{2,1,0:T(8,128)S(1)} %maximum_bitcast_fusion.1), channel_id=6, replica_groups=mesh['sp_0'=8,'sp_1'=4,'sp_2'=2,'tp'=4] {'sp_1'}, dimensions={0}, use_global_device_ids=true | all-gather | bytes 665600 | tf_op jit(solution)/shard_map/all_gather | solution.py:56
  79.7 0.7 maximum_bitcast_fusion.2
  85.7 13.2 %all-reduce.8 = s32[16]{0:T(128)S(1)} all-reduce(s32[16]{0:T(128)S(1)} %fusion.255), channel_id=4, replica_groups=mesh['sp_0'=8,'sp_1'=4,'sp_2'=2,'tp'=4] {'sp_0'}, use_global_device_ids=true, to_apply=%add.8 | all-reduce | flops 16 | bytes 128
  98.9 0.7 fusion.286
  116.1 2.3 all-gather.11.cloned.1.call-done
  118.4 0.8 fusion.281
  119.5 0.9 add_select_fusion.4
  120.7 1.4 fusion.280
  122.5 0.8 copy.155
  123.2 0.7 copy.154
  124.0 0.7 copy.153
  124.9 2.0 multiply_reduce_fusion
  127.5 3.9 all-to-all-start
  131.7 3.9 all-to-all-done
  135.6 1.7 convolution_convert_fusion
  137.6 21.7 %all_to_all.32 = bf16[4,512,512]{2,1,0:T(8,128)(2,1)S(1)} all-to-all(bf16[4,512,512]{2,1,0:T(8,128)(2,1)S(1)} %bitcast.689), channel_id=1, replica_groups=mesh['sp_0'=8,'sp_1'=4,'sp_2'=2,'tp'=4] {'tp'}, dimensions={0} | all-to-all | bytes 4194304 | tf_op jit(solution)/shard_map/all_to_all | solution.py:104
  159.5 0.7 copy-done.2
  161.2 3.2 all-to-all-start.2
  164.5 4.1 all-to-all-done.2
  169.0 1.5 broadcast_in_dim.112
  170.6 4.6 all-to-all-start.3
  175.2 16.9 %all-to-all-done.3 = bf16[4,512,512]{1,2,0:T(8,128)(2,1)} async-done(((bf16[4,512,512]{1,2,0:T(8,128)(2,1)}), bf16[4,512,512]{1,2,0:T(8,128)(2,1)}, u32[]{:S(2)}, u32[]{:S(2)}) %all-to-all-start.3) | async-done | bytes 2097184 | tf_op jit(solution)/shard_map/all_to_all | solution.py:21
  192.1 2.1 stack.2
  194.2 383.4 %all_to_all.33 = bf16[64,32,4096]{2,1,0:T(8,128)(2,1)} all-to-all(bf16[64,32,4096]{2,1,0:T(8,128)(2,1)S(1)} %stack.2), channel_id=1, replica_groups=mesh['sp_0'=8,'sp_1'=4,'sp_2'=2,'tp'=4] {'sp_0','sp_1','sp_2'}, dimensions={0} | all-to-all | bytes 33554432 | tf_op jit(solution)/shard_map/all_to_all | solution.py:16
  577.5 16.6 %fusion.24 = bf16[512,2048]{1,0:T(8,128)(2,1)} fusion(bf16[2048,4096]{1,0:T(8,128)(2,1)} %bitcast.687, bf16[512,2048]{0,1:T(8,128)(2,1)} %bitcast.142), kind=kOutput, calls=%fused_computation.56 | convolution fusion | flops 8594128896 | bytes 20971520 | tf_op jit(solution)/shard_map/dot_general | solution.py:276
  594.1 1.8 copy.230
  595.9 26.7 %all_to_all.34 = bf16[4,512,512]{2,1,0:T(8,128)(2,1)S(1)} all-to-all(bf16[4,512,512]{2,1,0:T(8,128)(2,1)S(1)} %bitcast.690), channel_id=1, replica_groups=mesh['sp_0'=8,'sp_1'=4,'sp_2'=2,'tp'=4] {'tp'}, dimensions={0} | all-to-all | bytes 4194304 | tf_op jit(solution)/shard_map/all_to_all | solution.py:104
  622.9 1.0 fusion.37
  (212 shorter events, 22.5 us)
Async XLA Ops:
  6.5 129.1 %copy-start = (bf16[256,2048]{1,0:T(8,128)(2,1)S(1)}, bf16[256,2048]{1,0:T(8,128)(2,1)}, u32[]{:S(2)}) copy-start(bf16[256,2048]{1,0:T(8,128)(2,1)} %param.26) | copy-start | bytes 3145732
  6.5 3.5 copy-start.5
  6.5 4.1 copy-start.6
  6.5 4.1 copy-start.7
  6.5 111.8 %all-gather.11.cloned.1.call-start = ((), (), s32[]{:S(2)}) async-start(), calls=%async_computation.6 | async-start | bytes 1216512 | tf_op jit(solution)/shard_map/all_gather | solution.py:56
  10.7 26.1 %copy-start.16 = (u32[256]{0:T(256)S(1)}, u32[256]{0:T(256)}, u32[]{:S(2)}) copy-start(u32[256]{0:T(256)} %constant.114) | copy-start | bytes 3076
  10.7 36.1 %copy-start.15 = (u32[256]{0:T(256)S(1)}, u32[256]{0:T(256)}, u32[]{:S(2)}) copy-start(u32[256]{0:T(256)} %constant.119) | copy-start | bytes 3076
  36.7 44.3 %copy-start.14 = (u32[256]{0:T(256)S(1)}, u32[256]{0:T(256)}, u32[]{:S(2)}) copy-start(u32[256]{0:T(256)} %constant.124) | copy-start | bytes 3076
  79.2 36.5 %copy-start.8 = (f32[2]{0:T(128)}, f32[2]{0:T(128)S(1)}, u32[]{:S(2)}) copy-start(f32[2]{0:T(128)S(1)} %get-tuple-element.374) | copy-start | bytes 28
  119.4 2.6 copy-start.11
  120.7 4.2 copy-start.9
  122.0 2.8 copy-start.12
  124.8 6.6 %copy-start.13 = (bf16[256]{0:T(256)(128)(2,1)S(1)}, bf16[256]{0:T(256)(128)(2,1)}, u32[]{:S(2)}) copy-start(bf16[256]{0:T(256)(128)(2,1)} %param.25) | copy-start | bytes 1540
  127.5 8.1 %all-to-all-start = ((f32[4,1,512]{2,1,0:T(1,128)}), f32[4,1,512]{2,1,0:T(1,128)S(1)}, u32[]{:S(2)}, u32[]{:S(2)}) async-start(f32[4,1,512]{2,1,0:T(1,128)} %broadcast_in_dim.110), calls=%async_computation | async-start | bytes 16384 | tf_op jit(solution)/shard_map/all_to_all | solution.py:21
  159.2 1.0 copy-start.2
  160.3 4.2 copy-start.10
  161.2 7.4 %all-to-all-start.2 = ((f32[4,1,512]{2,1,0:T(1,128)}), f32[4,1,512]{2,1,0:T(1,128)S(1)}, u32[]{:S(2)}, u32[]{:S(2)}) async-start(f32[4,1,512]{2,1,0:T(1,128)} %broadcast_in_dim.111), calls=%async_computation.2 | async-start | bytes 16384 | tf_op jit(solution)/shard_map/all_to_all | solution.py:21
  170.6 4.6 copy-start.3
  170.6 4.6 copy-start.4
  170.6 21.5 %all-to-all-start.3 = ((bf16[4,512,512]{1,2,0:T(8,128)(2,1)}), bf16[4,512,512]{1,2,0:T(8,128)(2,1)}, u32[]{:S(2)}, u32[]{:S(2)}) async-start(bf16[4,512,512]{1,2,0:T(8,128)(2,1)} %broadcast_in_dim.112), calls=%async_computation.3 | async-start | bytes 4194304 | tf_op jit(solution)/shard_map/all_to_all | solution.py:21
  595.9 27.9 %copy-start.1 = (bf16[256,2048]{1,0:T(8,128)(2,1)S(1)}, bf16[256,2048]{1,0:T(8,128)(2,1)}, u32[]{:S(2)}) copy-start(bf16[256,2048]{1,0:T(8,128)(2,1)} %param.26) | copy-start | bytes 3145732
Sparse Core Ops, SparseCore 0:
  80.5 37.8 all-gather.10
